TPU v7x, 512 devices: a whole 4x8x8 slice. The times are simulated.
512 devices in a mesh: ep: 32 (over z, x), tp: 16 (over y, core).
Axes of the slice: x: 4, y: 8, z: 8, core: 2. Of those that a mesh axis runs over, the one named last changes fastest.
Arguments:
- mixer_in: bfloat16 [4096, 2048], P('ep'), may hold values from -6 to 6
- mixer_gain: float32 [2048], replicated, may hold values from 0.1 to 1.9
- w_value: bfloat16 [2048, 1536], P(None, 'tp'), may hold values from -0.125 to 0.125
- w_gate: bfloat16 [2048, 1536], P(None, 'tp'), may hold values from -0.125 to 0.125
- w_taps: float32 [31, 1536], P(None, 'tp'), may hold values from -3 to 3
- channel_gain: float32 [1536], P('tp'), may hold values from 0.1 to 1.9
- w_output: bfloat16 [1536, 2048], P('tp'), may hold values from -0.15625 to 0.15625
- expert_in: bfloat16 [4096, 2048], P('ep'), may hold values from -6 to 6
- expert_gain: float32 [2048], replicated, may hold values from 0 to 8
- route_experts: int32 [4096, 4], P('ep'), may hold values from 0 to 31, all different within a row; in each aligned block of 128 rows (0 to 127, 128 to 255, ...) at most 32 rows name the same one
- route_scores: float32 [4096, 4], P('ep'), may hold values from -6 to 6
- expert_gate: bfloat16 [32, 2048, 2048], P('ep', None, 'tp'), may hold values from -0.125 to 0.125
- expert_up: bfloat16 [32, 2048, 2048], P('ep', None, 'tp'), may hold values from -0.125 to 0.125
- expert_down: bfloat16 [32, 2048, 2048], P('ep', 'tp'), may hold values from -0.125 to 0.125
Outputs:
- mixer_out: bfloat16 [4096, 2048], P('ep')
- expert_out: bfloat16 [4096, 2048], P('ep')
Inputs may be any that keep to these rules, and one draw needn't show every extreme that they name: `route_experts`: each row names 4 different experts. In each aligned block of 128 rows (the rows of one index of ep) no expert is named more than 32 times, a bound that some block reaches.
All inputs are finite; a program needn't handle non-finite values.
Results may differ from a plain program's by a relative error of at most 0.02.
Values may be sent and summed in bfloat16 or wider, within the bound.
No kernel may reach another device: no remote copies, remote signals or barrier semaphores. Data moves between devices by JAX's collectives and lax.ppermute only.
A program may use at most 64 MiB of HBM per device.

v0:
```python
import jax
import jax.numpy as jnp
from jax import lax
from jax.sharding import Mesh
from jax.sharding import PartitionSpec as P

CONV_CH = 1536
CONV_W = 31
TOP_K = 4
TP = ("tp_0", "tp_1")
epsilon = 1e-05
clamp_limit = 7.0
swish_slope = 1.702


def shifted(block, axis, distance):
    devices = range(lax.axis_size(axis))
    route = [(i - distance, i) for i in devices if i - distance in devices]
    return lax.ppermute(block, axis, route)


def sent_to_all(x, axis):
    copies = jnp.broadcast_to(x, (lax.axis_size(axis), *x.shape))
    return lax.all_to_all(copies, axis, split_axis=0, concat_axis=0, tiled=True)


def over_copies(x, axis):
    everything = sent_to_all(x, axis)
    return jnp.sum(everything, axis=0)


def packed_total(arrays, axis):
    line, at, done = (jnp.concatenate([a.reshape(-1) for a in arrays]), 0, [])
    subtotal = over_copies(line, axis)
    for a in arrays:
        done.append(subtotal[at : at + a.size].reshape(a.shape))
        at += a.size
    return tuple(done)


def by_axis(x, axes):
    for axis in axes:
        x = lax.psum(x, axis)
    return x


def row_norm(inputs, gains):
    widened = inputs.astype(jnp.float32)
    row_mean = jnp.mean(widened, axis=-1, keepdims=True)
    row_var = jnp.mean(jnp.square(widened - row_mean), axis=-1, keepdims=True)
    return (widened - row_mean) * lax.rsqrt(row_var + epsilon) * gains


def local(
    mixer_in,
    mixer_gain,
    w_value,
    w_gate,
    w_taps,
    channel_gain,
    w_output,
    expert_in,
    expert_gain,
    route_experts,
    route_scores,
    expert_gate,
    expert_up,
    expert_down,
):
    normed = row_norm(mixer_in, mixer_gain).astype(jnp.bfloat16)
    values = jnp.dot(normed, w_value, preferred_element_type=jnp.float32)
    gate_pre = jnp.dot(normed, w_gate, preferred_element_type=jnp.float32)
    gated_values = (values * jax.nn.sigmoid(gate_pre)).astype(jnp.bfloat16)
    mixer_rows = gated_values.shape[0]
    reach_rows = CONV_W - 1
    earlier = shifted(gated_values[mixer_rows - reach_rows :], "ep", 1)
    extended = jnp.concatenate([earlier, gated_values], axis=0)
    conv_out = jnp.zeros(gated_values.shape, jnp.float32)
    for offset in range(CONV_W):
        conv_out = (
            conv_out + extended[offset : offset + mixer_rows].astype(jnp.float32) * w_taps[offset]
        )
    channel_sums = packed_total(
        (
            jnp.sum(conv_out, axis=1, keepdims=True),
            jnp.sum(conv_out * conv_out, axis=1, keepdims=True),
        ),
        TP,
    )
    row_mean = channel_sums[0] / CONV_CH
    row_var = channel_sums[1] / CONV_CH - row_mean * row_mean
    activated = jax.nn.silu(
        (conv_out - row_mean) * lax.rsqrt(row_var + epsilon) * channel_gain
    ).astype(jnp.bfloat16)
    mixer_out = (
        by_axis(
            jnp.dot(activated, w_output, preferred_element_type=jnp.float32).astype(jnp.bfloat16),
            TP,
        )
        .astype(jnp.float32)
        .astype(jnp.bfloat16)
    )
    rows_b = expert_in.shape[0]
    width = expert_in.shape[1]
    experts = lax.axis_size("ep")
    capacity = 2 * rows_b * TOP_K // experts
    slot_share = capacity // lax.axis_size(TP)
    column = lax.axis_index(TP)
    normed_b = row_norm(expert_in, expert_gain).astype(jnp.bfloat16)
    raised = jnp.exp(route_scores)
    route_weights = raised / jnp.sum(raised, axis=1, keepdims=True)
    flat_ids = route_experts.reshape(-1)
    onehot = (flat_ids[:, None] == jnp.arange(experts, dtype=jnp.int32)[None, :]).astype(jnp.int32)
    slot_index = jnp.sum((jnp.cumsum(onehot, axis=0) - onehot) * onehot, axis=1)
    owner_row = jnp.arange(rows_b * TOP_K, dtype=jnp.int32) // TOP_K
    slot_table = (
        jnp.full((capacity * experts,), rows_b, jnp.int32)
        .at[slot_index * experts + flat_ids]
        .set(owner_row)
    )
    padded = jnp.concatenate([normed_b, jnp.zeros((1, width), jnp.bfloat16)], axis=0)
    gate_w = expert_gate[0]
    up_w = expert_up[0]
    down_w = expert_down[0]
    own_table = lax.dynamic_slice_in_dim(
        slot_table, column * slot_share * experts, slot_share * experts
    )
    sending = jnp.take(padded, own_table, axis=0).reshape(slot_share, experts, width)
    arrived = lax.all_to_all(sending, "ep", split_axis=1, concat_axis=1, tiled=True)
    block_rows = lax.all_gather(arrived, TP, axis=0, tiled=True)
    flat_rows = block_rows.reshape(block_rows.shape[0] * block_rows.shape[1], block_rows.shape[2])
    gate_e = jnp.minimum(
        jnp.dot(flat_rows, gate_w, preferred_element_type=jnp.float32), clamp_limit
    )
    up_e = jnp.clip(
        jnp.dot(flat_rows, up_w, preferred_element_type=jnp.float32), -clamp_limit, clamp_limit
    )
    hidden = (
        ((up_e + 1.0) * gate_e * jax.nn.sigmoid(swish_slope * gate_e))
        .astype(jnp.bfloat16)
        .reshape(block_rows.shape[0], block_rows.shape[1], gate_w.shape[1])
        .reshape(capacity * experts, gate_w.shape[1])
    )
    summed = lax.psum_scatter(
        jnp.dot(hidden, down_w, preferred_element_type=jnp.float32).astype(jnp.bfloat16),
        TP,
        scatter_dimension=0,
        tiled=True,
    )
    returned = lax.all_to_all(
        summed.reshape(slot_share, experts, width), "ep", split_axis=1, concat_axis=1, tiled=True
    )
    every_slot = lax.all_gather(returned, TP, axis=0, tiled=True).reshape(capacity * experts, width)
    picked = jnp.take(every_slot, slot_index * experts + flat_ids, axis=0)
    picked = picked.reshape(rows_b, TOP_K, width).astype(jnp.float32)
    expert_out = jnp.sum(picked * route_weights[:, :, None], axis=1).astype(jnp.bfloat16)
    return (mixer_out, expert_out)


def solution(mesh):
    split = Mesh(mesh.devices.reshape(mesh.shape["ep"], 8, 2), ("ep", "tp_0", "tp_1"))
    in_specs = (
        P("ep", None),
        P(),
        P(None, TP),
        P(None, TP),
        P(None, TP),
        P(TP),
        P(TP, None),
        P("ep", None),
        P(),
        P("ep", None),
        P("ep", None),
        P("ep", None, TP),
        P("ep", None, TP),
        P("ep", TP, None),
    )
    out_specs = (P("ep", None), P("ep", None))
    return jax.shard_map(local, mesh=split, in_specs=in_specs, out_specs=out_specs, check_vma=False)
```

profile of v0, /device:TPU:1, one launch (start us, length us, event | category | flops | bytes accessed | tf_op | source)
XLA Modules:
  0.0 251.4 jit_solution(10205323536202366580)
XLA Ops:
  8.1 0.9 copy.59
  9.3 1.2 reduce-window.6
  10.9 2.4 scatter_custom_fusion
  13.4 1.2 convert_reduce_fusion
  14.6 1.3 fusion.13
  16.2 1.4 fusion.15
  17.6 0.7 gather_fusion
  18.4 0.3 broadcast_select_fusion
  18.7 24.8 %all_to_all.16 = bf16[2,32,2048]{2,0,1:T(2,128)(2,1)S(1)} all-to-all(bf16[2,32,2048]{2,0,1:T(2,128)(2,1)S(1)} %broadcast_select_fusion), channel_id=1, replica_groups=mesh['ep'=32,'tp_0'=8,'tp_1'=2] {'ep'}, dimensions={1} | all-to-all | bytes 524288 | tf_op jit(solution)/shard_map/all_to_all | solution.py:129
  43.6 0.8 copy.67
  44.4 42.1 %all-gather.3.cloned.1.call-done = bf16[32,32,2048]{2,1,0:T(8,128)(2,1)} async-done(((bf16[2,32,2048]{2,1,0:T(8,128)(2,1)}), bf16[32,32,2048]{2,1,0:T(8,128)(2,1)}) %all-gather.3.cloned.1.call-update) | async-done | bytes 4194320 | tf_op jit(solution)/shard_map/all_gather | solution.py:130
  86.5 3.4 %convolution_minimum_fusion = f32[1024,128]{1,0:T(8,128)S(1)} fusion(bf16[1024,2048]{1,0:T(8,128)(2,1)} %bitcast.103, bf16[1,2048,128]{2,1,0:T(8,128)(2,1)S(1)} %copy-done.8), kind=kOutput, calls=%fused_computation.14 | convolution fusion | flops 537001984 | bytes 5242880 | tf_op jit(solution)/shard_map/dot_general | solution.py:133
  90.0 8.5 %convolution_convert_fusion = bf16[1024,2048]{1,0:T(8,128)(2,1)} fusion(f32[1024,128]{1,0:T(8,128)S(1)} %convolution_minimum_fusion, bf16[1024,2048]{1,0:T(8,128)(2,1)} %bitcast.104, bf16[1,128,2048]{2,1,0:T(8,128)(2,1)S(1)} %copy-done, bf16[1,2048,128]{2,1,0:T(8,128)(2,1)S(1)} %copy-done.2), kind=kOutput, calls=%fused_computation.4 | convolution fusion | flops 1077018624 | bytes 9961472 | tf_op jit(solution)/shard_map/dot_general | solution.py:145
  98.6 0.9 copy-done.1
  99.7 0.3 fusion.16
  100.0 0.4 fusion.80
  100.4 0.4 fusion.12
  100.9 3.1 %collective-permute-start = (bf16[30,96]{0,1:T(8,128)(2,1)S(1)}, bf16[30,96]{0,1:T(8,128)(2,1)S(1)}, u32[]{:S(2)}, u32[]{:S(2)}) collective-permute-start(bf16[30,96]{0,1:T(8,128)(2,1)S(1)} %slice.268), channel_id=1, source_target_pairs={{0,16},{16,32},{32,48},{48,64},{64,80},{80,96},{96,112},{112,128},... | collective-permute-start | bytes 17288 | tf_op jit(solution)/shard_map/ppermute | solution.py:19
  104.1 0.9 collective-permute-done
  104.9 0.9 fusion.82
  105.8 12.5 %all_to_all.17 = f32[16,1,256]{2,1,0:T(1,128)S(1)} all-to-all(f32[16,1,256]{2,1,0:T(1,128)S(1)} %broadcast_in_dim.42), channel_id=1, replica_groups=mesh['ep'=32,'tp_0'=8,'tp_1'=2] {'tp_0','tp_1'}, dimensions={0} | all-to-all | bytes 32768 | tf_op jit(solution)/shard_map/all_to_all | solution.py:24
  118.4 1.2 convolution_convert_fusion.1
  119.6 42.9 %reduce-scatter.2.cloned.1.call-done = bf16[64,2048]{1,0:T(8,128)(2,1)} async-done(((bf16[1024,2048]{1,0:T(8,128)(2,1)}), bf16[64,2048]{1,0:T(8,128)(2,1)}) %reduce-scatter.2.cloned.1.call-update) | async-done | bytes 262160 | tf_op jit(solution)/shard_map/reduce_scatter | solution.py:144
  162.5 1.2 copy.68
  163.8 18.9 %all_to_all.18 = bf16[2,32,2048]{2,0,1:T(2,128)(2,1)S(1)} all-to-all(bf16[2,32,2048]{2,0,1:T(2,128)(2,1)S(1)} %copy.68), channel_id=1, replica_groups=mesh['ep'=32,'tp_0'=8,'tp_1'=2] {'ep'}, dimensions={1} | all-to-all | bytes 524288 | tf_op jit(solution)/shard_map/all_to_all | solution.py:150
  182.7 0.8 copy.69
  184.2 9.5 %all-reduce.4.cloned.1.call-done = bf16[128,2048]{1,0:T(8,128)(2,1)} async-done(((bf16[128,2048]{1,0:T(8,128)(2,1)}), bf16[128,2048]{1,0:T(8,128)(2,1)}) %all-reduce.4.cloned.1.call-update) | async-done | bytes 524304 | tf_op jit(solution)/shard_map/psum | solution.py:43
  193.8 32.8 %all-gather.5.cloned.1.call-done = bf16[32,32,2048]{2,1,0:T(8,128)(2,1)} async-done(((bf16[2,32,2048]{2,1,0:T(8,128)(2,1)}), bf16[32,32,2048]{2,1,0:T(8,128)(2,1)}) %all-gather.5.cloned.1.call-update) | async-done | bytes 4194320 | tf_op jit(solution)/shard_map/all_gather | solution.py:153
  226.6 7.1 %gather_fusion.1 = bf16[512,2048]{1,0:T(8,128)(2,1)S(1)} fusion(bf16[1024,2048]{1,0:T(8,128)(2,1)} %bitcast.102, s32[1024]{0:T(1024)S(1)} %pad_clamp_fusion), kind=kCustom, calls=%fused_computation.1 | custom fusion | bytes 4196352 | tf_op jit(solution)/shard_map/jit(_take)/gather | solution.py:154
  233.7 2.2 gather.15
  236.0 6.4 %multiply_reduce_fusion = bf16[128,2048]{1,0:T(8,128)(2,1)} fusion(f32[128,4]{1,0:T(8,128)S(1)} %copy.70, bf16[128,4,2048]{2,1,0:T(4,128)(2,1)} %gather.15, pred[128,4]{1,0:T(8,128)(4,1)S(1)} %copy.63), kind=kLoop, calls=%fused_computation.3 | loop fusion | flops 3932160 | bytes 2624000 | tf_op jit(solution)/shard_map/reduce_sum | solution.py:156
  242.4 1.9 copy.79
  (70 shorter events, 2.4 us)
Async XLA Ops:
  8.0 82.0 %copy-start = (bf16[1,128,2048]{2,1,0:T(8,128)(2,1)S(1)}, bf16[1,128,2048]{2,1,0:T(8,128)(2,1)}, u32[]{:S(2)}) copy-start(bf16[1,128,2048]{2,1,0:T(8,128)(2,1)} %param.27) | copy-start | bytes 1572868
  8.0 78.5 %copy-start.8 = (bf16[1,2048,128]{2,1,0:T(8,128)(2,1)S(1)}, bf16[1,2048,128]{2,1,0:T(8,128)(2,1)}, u32[]{:S(2)}) copy-start(bf16[1,2048,128]{2,1,0:T(8,128)(2,1)} %param.25) | copy-start | bytes 1572868
  8.0 78.5 %all-gather.3.cloned.1.call-start = ((), (), s32[]{:S(2)}) async-start(), calls=%async_computation.6 | async-start | bytes 4456448 | tf_op jit(solution)/shard_map/all_gather | solution.py:130
  18.4 71.6 %copy-start.2 = (bf16[1,2048,128]{2,1,0:T(8,128)(2,1)S(1)}, bf16[1,2048,128]{2,1,0:T(8,128)(2,1)}, u32[]{:S(2)}) copy-start(bf16[1,2048,128]{2,1,0:T(8,128)(2,1)} %param.26) | copy-start | bytes 1572868
  44.4 118.2 %reduce-scatter.2.cloned.1.call-start = ((), (), s32[]{:S(2)}) async-start(), calls=%async_computation.7 | async-start | bytes 4456448 | tf_op jit(solution)/shard_map/reduce_scatter | solution.py:144
  98.5 1.0 copy-start.1
  98.5 1.5 copy-start.9
  98.5 1.5 copy-start.11
  98.5 1.9 copy-start.10
  98.5 5.5 %copy-start.4 = (f32[31,96]{1,0:T(8,128)S(1)}, f32[31,96]{1,0:T(8,128)}, u32[]{:S(2)}) copy-start(f32[31,96]{1,0:T(8,128)} %param.18) | copy-start | bytes 35716
  98.5 19.9 %copy-start.3 = (bf16[96,2048]{1,0:T(8,128)(2,1)S(1)}, bf16[96,2048]{1,0:T(8,128)(2,1)}, u32[]{:S(2)}) copy-start(bf16[96,2048]{1,0:T(8,128)(2,1)} %param.20) | copy-start | bytes 1179652
  98.5 19.8 %copy-start.7 = (f32[96]{0:T(128)S(1)}, f32[96]{0:T(128)}, u32[]{:S(2)}) copy-start(f32[96]{0:T(128)} %param.19) | copy-start | bytes 1156
  98.5 85.3 %copy-start.5 = (s32[128,4]{0,1:T(4,128)S(1)}, s32[128,4]{0,1:T(4,128)}, u32[]{:S(2)}) copy-start(s32[128,4]{0,1:T(4,128)} %param.23) | copy-start | bytes 6148
  98.6 85.5 %copy-start.6 = (f32[128,4]{0,1:T(4,128)S(1)}, f32[128,4]{0,1:T(4,128)}, u32[]{:S(2)}) copy-start(f32[128,4]{0,1:T(4,128)} %param.24) | copy-start | bytes 6148
  98.6 95.1 %all-reduce.4.cloned.1.call-start = ((), (), s32[]{:S(2)}) async-start(), calls=%async_computation.4 | async-start | bytes 1048576 | tf_op jit(solution)/shard_map/psum | solution.py:43
  100.9 4.0 %collective-permute-start = (bf16[30,96]{0,1:T(8,128)(2,1)S(1)}, bf16[30,96]{0,1:T(8,128)(2,1)S(1)}, u32[]{:S(2)}, u32[]{:S(2)}) collective-permute-start(bf16[30,96]{0,1:T(8,128)(2,1)S(1)} %slice.268), channel_id=1, source_target_pairs={{0,16},{16,32},{32,48},{48,64},{64,80},{80,96},{96,112},{112,128},... | collective-permute-start | bytes 17288 | tf_op jit(solution)/shard_map/ppermute | solution.py:19
  119.6 107.0 %all-gather.5.cloned.1.call-start = ((), (), s32[]{:S(2)}) async-start(), calls=%async_computation.8 | async-start | bytes 4456448 | tf_op jit(solution)/shard_map/all_gather | solution.py:153
  183.5 58.9 %all-reduce.6.cloned.1.call-start = ((), (), s32[]{:S(2)}) async-start(), calls=%async_computation.5 | async-start | bytes 1048576 | tf_op jit(solution)/shard_map/psum | solution.py:43
Sparse Core Ops, SparseCore 0:
  44.5 42.0 all-gather.2
  98.7 63.8 reduce-scatter.1
  183.6 42.9 all-gather.4
Sparse Core Ops, SparseCore 1:
  119.7 74.0 all-reduce.3
  196.5 39.0 all-reduce.5
where the time goes:
time: 252 us; the launch traced here: 251 us
  waiting for transfers between devices  128 us (51%)
  blocking collectives  56.2 us (22%)
  local copies, waits for them, and re-layouts  20.4 us (8%)
  between operations  15.5 us (6%)
  matrix products  13.9 us (6%)
  other arithmetic  13.6 us (5%)
  starting transfers between devices  3.48 us (1%)
    reduce_scatter x1, waiting for transfers between devices, local(): lax.psum_scatter(jnp.dot(hidden, down_w, preferred_element_type=jnp.float...  42.9 us
    all_gather x1, waiting for transfers between devices, local(): block_rows = lax.all_gather(arrived, TP, axis=0, tiled=True)  42.1 us
    all_gather x1, waiting for transfers between devices, local(): lax.all_gather(returned, TP, axis=0, tiled=True)  32.8 us
    all_to_all x1, blocking collectives, local(): lax.all_to_all(sending, 'ep', split_axis=1, concat_axis=1, tiled=True)  24.8 us
    all_to_all x1, blocking collectives, local(): lax.all_to_all(summed.reshape(slot_share, experts, width), 'ep', split_ax...  18.9 us
    all_to_all x1, blocking collectives, sent_to_all(): return lax.all_to_all(copies, axis, split_axis=0, concat_axis=0, tiled=True)  12.5 us
    psum x2, waiting for transfers between devices, by_axis(): x = lax.psum(x, axis)  9.51 us
    gather x2, local copies, waits for them, and re-layouts, local(): picked = jnp.take(every_slot, slot_index * experts + flat_ids, axis=0)  9.37 us
  transfers between devices with their start and end apart: 6, of which 5 were waited for; matrix products, arithmetic and copies ran while one was open for 9% of the time, Pallas kernels for 0%

commit v1 on v0

--- a/solution.py
+++ b/solution.py
@@ -150,7 +150,9 @@
     returned = lax.all_to_all(
         summed.reshape(slot_share, experts, width), "ep", split_axis=1, concat_axis=1, tiled=True
     )
-    every_slot = lax.all_gather(returned, TP, axis=0, tiled=True).reshape(capacity * experts, width)
+    every_slot = jnp.concatenate(
+        lax.all_to_all(jnp.stack([returned] * lax.axis_size(TP)), TP, 0, 0), axis=0
+    ).reshape(capacity * experts, width)
     picked = jnp.take(every_slot, slot_index * experts + flat_ids, axis=0)
     picked = picked.reshape(rows_b, TOP_K, width).astype(jnp.float32)
     expert_out = jnp.sum(picked * route_weights[:, :, None], axis=1).astype(jnp.bfloat16)

time: 252 us -> 363 us (1.44)
  waiting for transfers between devices: 128 us -> 243 us
  blocking collectives: 56.2 us -> 24.8 us
  starting transfers between devices: 3.48 us -> 27.2 us
    psum x2, waiting for transfers between devices: 9.51 us -> 127 us  [by_axis(): x = lax.psum(x, axis)]
    all_gather x1 -> x0, waiting for transfers between devices: 32.8 us -> none  [local(): lax.all_gather(returned, TP, axis=0, tiled=True)]
    all_to_all x2 -> x0, blocking collectives: 31.4 us -> none  [the longest x1 18.9 us: local(): lax.all_to_all(summed.reshape(slot_share, experts, width), 'ep', split_ax...]
    all_to_all x0 -> x3, starting transfers between devices: none -> 23.8 us  [the longest x1 9.88 us: sent_to_all(): return lax.all_to_all(copies, axis, split_axis=0, concat_axis=0, tiled=True)]
    all_to_all x0 -> x3, waiting for transfers between devices: none -> 16.8 us  [the longest x1 9.57 us: local(): lax.all_to_all(summed.reshape(slot_share, experts, width), 'ep', split_ax...]
    reduce_scatter x1, waiting for transfers between devices: 42.9 us -> 56.7 us  [local(): lax.psum_scatter(jnp.dot(hidden, down_w, preferred_element_type=jnp.float...]
  transfers between devices with their start and end apart: 6 -> 8, of which waited for: 5 -> 6; matrix products, arithmetic and copies ran while one was open for 9% -> 6% of each run, Pallas kernels for 0% -> 0%
where the time goes in v1:
time: 363 us; the launch traced here: 362 us
  waiting for transfers between devices  243 us (67%)
  starting transfers between devices  27.2 us (7%)
  blocking collectives  24.8 us (7%)
  local copies, waits for them, and re-layouts  23.6 us (7%)
  between operations  15.8 us (4%)
  matrix products  13.9 us (4%)
  other arithmetic  13.6 us (4%)
    psum x2, waiting for transfers between devices, by_axis(): x = lax.psum(x, axis)  127 us
    reduce_scatter x1, waiting for transfers between devices, local(): lax.psum_scatter(jnp.dot(hidden, down_w, preferred_element_type=jnp.float...  56.7 us
    all_gather x1, waiting for transfers between devices, local(): block_rows = lax.all_gather(arrived, TP, axis=0, tiled=True)  42.1 us
    all_to_all x1, blocking collectives, local(): lax.all_to_all(sending, 'ep', split_axis=1, concat_axis=1, tiled=True)  24.8 us
    all_to_all x1, starting transfers between devices, sent_to_all(): return lax.all_to_all(copies, axis, split_axis=0, concat_axis=0, tiled=True)  9.88 us
    all_to_all x1, waiting for transfers between devices, local(): lax.all_to_all(summed.reshape(slot_share, experts, width), 'ep', split_ax...  9.57 us
    gather x2, local copies, waits for them, and re-layouts, local(): picked = jnp.take(every_slot, slot_index * experts + flat_ids, axis=0)  9.37 us
    all_to_all x1, starting transfers between devices, local(): lax.all_to_all(summed.reshape(slot_share, experts, width), 'ep', split_ax...  9.1 us
  transfers between devices with their start and end apart: 8, of which 6 were waited for; matrix products, arithmetic and copies ran while one was open for 6% of the time, Pallas kernels for 0%

profile of v1, /device:TPU:1, one launch (start us, length us, event | category | flops | bytes accessed | tf_op | source)
XLA Modules:
  0.0 362.1 jit_solution(1157227760470907698)
XLA Ops:
  8.1 0.9 copy.59
  9.3 1.2 reduce-window.6
  10.9 2.4 scatter_custom_fusion
  13.4 1.2 convert_reduce_fusion
  14.6 1.3 fusion.13
  16.2 1.4 fusion.15
  17.6 0.7 gather_fusion
  18.7 24.8 %all_to_all.21 = bf16[2,32,2048]{2,0,1:T(2,128)(2,1)S(1)} all-to-all(bf16[2,32,2048]{2,0,1:T(2,128)(2,1)S(1)} %broadcast_select_fusion), channel_id=1, replica_groups=mesh['ep'=32,'tp_0'=8,'tp_1'=2] {'ep'}, dimensions={1} | all-to-all | bytes 524288 | tf_op jit(solution)/shard_map/all_to_all | solution.py:129
  43.6 0.8 copy.67
  44.4 42.1 %all-gather.2.cloned.1.call-done = bf16[32,32,2048]{2,1,0:T(8,128)(2,1)} async-done(((bf16[2,32,2048]{2,1,0:T(8,128)(2,1)}), bf16[32,32,2048]{2,1,0:T(8,128)(2,1)}) %all-gather.2.cloned.1.call-update) | async-done | bytes 4194320 | tf_op jit(solution)/shard_map/all_gather | solution.py:130
  86.5 3.4 convolution_minimum_fusion
  90.0 8.5 %convolution_convert_fusion = bf16[1024,2048]{1,0:T(8,128)(2,1)} fusion(f32[1024,128]{1,0:T(8,128)S(1)} %convolution_minimum_fusion, bf16[1024,2048]{1,0:T(8,128)(2,1)} %bitcast.103, bf16[1,128,2048]{2,1,0:T(8,128)(2,1)S(1)} %copy-done, bf16[1,2048,128]{2,1,0:T(8,128)(2,1)S(1)} %copy-done.2), kind=kOutput, calls=%fused_computation.4 | convolution fusion | flops 1077018624 | bytes 9961472 | tf_op jit(solution)/shard_map/dot_general | solution.py:145
  98.5 1.0 copy-done.1
  100.4 0.4 fusion.12
  100.9 3.1 collective-permute-start
  104.1 56.7 %reduce-scatter.2.cloned.1.call-done = bf16[64,2048]{1,0:T(8,128)(2,1)} async-done(((bf16[1024,2048]{1,0:T(8,128)(2,1)}), bf16[64,2048]{1,0:T(8,128)(2,1)}) %reduce-scatter.2.cloned.1.call-update) | async-done | bytes 262160 | tf_op jit(solution)/shard_map/reduce_scatter | solution.py:144
  160.8 1.9 copy.68
  162.7 9.1 %all-to-all-start.2 = ((bf16[2,32,2048]{2,0,1:T(2,128)(2,1)}), bf16[2,32,2048]{2,0,1:T(2,128)(2,1)S(1)}, u32[]{:S(2)}, u32[]{:S(2)}) async-start(bf16[2,32,2048]{2,0,1:T(2,128)(2,1)} %copy.68), calls=%async_computation.3 | async-start | bytes 524288 | tf_op jit(solution)/shard_map/all_to_all | solution.py:150
  171.8 0.9 fusion.82
  172.7 9.6 %all-to-all-done.2 = bf16[2,32,2048]{2,0,1:T(2,128)(2,1)S(1)} async-done(((bf16[2,32,2048]{2,0,1:T(2,128)(2,1)}), bf16[2,32,2048]{2,0,1:T(2,128)(2,1)S(1)}, u32[]{:S(2)}, u32[]{:S(2)}) %all-to-all-start.2) | async-done | bytes 262176 | tf_op jit(solution)/shard_map/all_to_all | solution.py:150
  182.3 0.6 broadcast_in_dim.42
  182.9 9.9 %all-to-all-start = ((f32[16,1,256]{2,1,0:T(1,128)}), f32[16,1,256]{2,1,0:T(1,128)S(1)}, u32[]{:S(2)}, u32[]{:S(2)}) async-start(f32[16,1,256]{2,1,0:T(1,128)} %broadcast_in_dim.42), calls=%async_computation | async-start | bytes 32768 | tf_op jit(solution)/shard_map/all_to_all | solution.py:24
  192.9 7.3 %all-to-all-done = f32[16,1,256]{2,1,0:T(1,128)S(1)} async-done(((f32[16,1,256]{2,1,0:T(1,128)}), f32[16,1,256]{2,1,0:T(1,128)S(1)}, u32[]{:S(2)}, u32[]{:S(2)}) %all-to-all-start) | async-done | bytes 16416 | tf_op jit(solution)/shard_map/all_to_all | solution.py:24
  200.1 2.5 stack.2
  202.6 4.8 %all-to-all-start.3 = ((bf16[16,2,32,2048]{3,2,1,0:T(8,128)(2,1)}), bf16[16,2,32,2048]{3,2,1,0:T(8,128)(2,1)}, u32[]{:S(2)}, u32[]{:S(2)}) async-start(bf16[16,2,32,2048]{3,2,1,0:T(8,128)(2,1)} %stack.2), calls=%async_computation.4 | async-start | bytes 8388608 | tf_op jit(solution)/shard_map/all_to_all | solution.py:154
  207.7 1.2 convolution_convert_fusion.1
  209.5 106.4 %all-reduce.4.cloned.1.call-done = bf16[128,2048]{1,0:T(8,128)(2,1)} async-done(((bf16[128,2048]{1,0:T(8,128)(2,1)}), bf16[128,2048]{1,0:T(8,128)(2,1)}) %all-reduce.4.cloned.1.call-update) | async-done | bytes 524304 | tf_op jit(solution)/shard_map/psum | solution.py:43
  316.0 7.1 %gather_fusion.1 = bf16[512,2048]{1,0:T(8,128)(2,1)S(1)} fusion(bf16[1024,2048]{1,0:T(8,128)(2,1)} %bitcast.40, s32[1024]{0:T(1024)S(1)} %pad_clamp_fusion), kind=kCustom, calls=%fused_computation.1 | custom fusion | bytes 4196352 | tf_op jit(solution)/shard_map/jit(_take)/gather | solution.py:156
  323.1 2.2 gather.15
  325.3 6.4 %multiply_reduce_fusion = bf16[128,2048]{1,0:T(8,128)(2,1)} fusion(f32[128,4]{1,0:T(8,128)S(1)} %copy.70, bf16[128,4,2048]{2,1,0:T(4,128)(2,1)} %gather.15, pred[128,4]{1,0:T(8,128)(4,1)S(1)} %copy.63), kind=kLoop, calls=%fused_computation.3 | loop fusion | flops 3932160 | bytes 2624000 | tf_op jit(solution)/shard_map/reduce_sum | solution.py:158
  331.8 21.0 %all-reduce.6.cloned.1.call-done = bf16[128,2048]{1,0:T(8,128)(2,1)} async-done(((bf16[128,2048]{1,0:T(8,128)(2,1)}), bf16[128,2048]{1,0:T(8,128)(2,1)}) %all-reduce.6.cloned.1.call-update) | async-done | bytes 524304 | tf_op jit(solution)/shard_map/psum | solution.py:43
  352.8 1.9 copy.79
  (72 shorter events, 3.5 us)
Async XLA Ops:
  8.0 82.0 %copy-start = (bf16[1,128,2048]{2,1,0:T(8,128)(2,1)S(1)}, bf16[1,128,2048]{2,1,0:T(8,128)(2,1)}, u32[]{:S(2)}) copy-start(bf16[1,128,2048]{2,1,0:T(8,128)(2,1)} %param.27) | copy-start | bytes 1572868
  8.0 78.5 %copy-start.8 = (bf16[1,2048,128]{2,1,0:T(8,128)(2,1)S(1)}, bf16[1,2048,128]{2,1,0:T(8,128)(2,1)}, u32[]{:S(2)}) copy-start(bf16[1,2048,128]{2,1,0:T(8,128)(2,1)} %param.25) | copy-start | bytes 1572868
  8.0 78.5 %all-gather.2.cloned.1.call-start = ((), (), s32[]{:S(2)}) async-start(), calls=%async_computation.7 | async-start | bytes 4456448 | tf_op jit(solution)/shard_map/all_gather | solution.py:130
  18.4 71.6 %copy-start.2 = (bf16[1,2048,128]{2,1,0:T(8,128)(2,1)S(1)}, bf16[1,2048,128]{2,1,0:T(8,128)(2,1)}, u32[]{:S(2)}) copy-start(bf16[1,2048,128]{2,1,0:T(8,128)(2,1)} %param.26) | copy-start | bytes 1572868
  44.4 116.4 %reduce-scatter.2.cloned.1.call-start = ((), (), s32[]{:S(2)}) async-start(), calls=%async_computation.8 | async-start | bytes 4456448 | tf_op jit(solution)/shard_map/reduce_scatter | solution.py:144
  98.5 1.0 copy-start.1
  98.5 1.5 copy-start.9
  98.5 1.5 copy-start.11
  98.5 1.9 copy-start.10
  98.5 5.5 %copy-start.4 = (f32[31,96]{1,0:T(8,128)S(1)}, f32[31,96]{1,0:T(8,128)}, u32[]{:S(2)}) copy-start(f32[31,96]{1,0:T(8,128)} %param.18) | copy-start | bytes 35716
  100.9 70.9 %collective-permute-start = (bf16[30,96]{0,1:T(8,128)(2,1)S(1)}, bf16[30,96]{0,1:T(8,128)(2,1)S(1)}, u32[]{:S(2)}, u32[]{:S(2)}) collective-permute-start(bf16[30,96]{0,1:T(8,128)(2,1)S(1)} %slice.268), channel_id=1, source_target_pairs={{0,16},{16,32},{32,48},{48,64},{64,80},{80,96},{96,112},{112,128},... | collective-permute-start | bytes 17288 | tf_op jit(solution)/shard_map/ppermute | solution.py:19
  162.7 19.6 %all-to-all-start.2 = ((bf16[2,32,2048]{2,0,1:T(2,128)(2,1)}), bf16[2,32,2048]{2,0,1:T(2,128)(2,1)S(1)}, u32[]{:S(2)}, u32[]{:S(2)}) async-start(bf16[2,32,2048]{2,0,1:T(2,128)(2,1)} %copy.68), calls=%async_computation.3 | async-start | bytes 524288 | tf_op jit(solution)/shard_map/all_to_all | solution.py:150
  182.9 17.2 %all-to-all-start = ((f32[16,1,256]{2,1,0:T(1,128)}), f32[16,1,256]{2,1,0:T(1,128)S(1)}, u32[]{:S(2)}, u32[]{:S(2)}) async-start(f32[16,1,256]{2,1,0:T(1,128)} %broadcast_in_dim.42), calls=%async_computation | async-start | bytes 32768 | tf_op jit(solution)/shard_map/all_to_all | solution.py:24
  202.6 5.1 %copy-start.3 = (bf16[96,2048]{1,0:T(8,128)(2,1)S(1)}, bf16[96,2048]{1,0:T(8,128)(2,1)}, u32[]{:S(2)}) copy-start(bf16[96,2048]{1,0:T(8,128)(2,1)} %param.20) | copy-start | bytes 1179652
  202.6 5.1 %copy-start.7 = (f32[96]{0:T(128)S(1)}, f32[96]{0:T(128)}, u32[]{:S(2)}) copy-start(f32[96]{0:T(128)} %param.19) | copy-start | bytes 1156
  202.6 6.6 %copy-start.5 = (s32[128,4]{0,1:T(4,128)S(1)}, s32[128,4]{0,1:T(4,128)}, u32[]{:S(2)}) copy-start(s32[128,4]{0,1:T(4,128)} %param.23) | copy-start | bytes 6148
  202.6 6.7 %copy-start.6 = (f32[128,4]{0,1:T(4,128)S(1)}, f32[128,4]{0,1:T(4,128)}, u32[]{:S(2)}) copy-start(f32[128,4]{0,1:T(4,128)} %param.24) | copy-start | bytes 6148
  202.6 113.3 %all-to-all-start.3 = ((bf16[16,2,32,2048]{3,2,1,0:T(8,128)(2,1)}), bf16[16,2,32,2048]{3,2,1,0:T(8,128)(2,1)}, u32[]{:S(2)}, u32[]{:S(2)}) async-start(bf16[16,2,32,2048]{3,2,1,0:T(8,128)(2,1)} %stack.2), calls=%async_computation.4 | async-start | bytes 8388608 | tf_op jit(solution)/shard_map/all_to_all | solution.py:154
  207.4 108.5 %all-reduce.4.cloned.1.call-start = ((), (), s32[]{:S(2)}) async-start(), calls=%async_computation.5 | async-start | bytes 1048576 | tf_op jit(solution)/shard_map/psum | solution.py:43
  208.9 143.8 %all-reduce.6.cloned.1.call-start = ((), (), s32[]{:S(2)}) async-start(), calls=%async_computation.6 | async-start | bytes 1048576 | tf_op jit(solution)/shard_map/psum | solution.py:43
Sparse Core Ops, SparseCore 0:
  44.5 42.0 all-gather.1
  98.6 62.0 reduce-scatter.1
Sparse Core Ops, SparseCore 1:
  210.8 105.1 all-reduce.3
  318.7 34.0 all-reduce.5
